TPU v7x, 32 devices: a whole 2x2x4 slice. The times are simulated.
32 devices in a mesh: grp: 2 (over y), fs: 4 (over z), tp: 4 (over x, core).
Axes of the slice: x: 2, y: 2, z: 4, core: 2. Of those that a mesh axis runs over, the one named last changes fastest.
Arguments:
- tokens: bfloat16 [8, 384, 2048], P(('grp', 'fs'), None, 'tp'), parts along dimension 0, may hold values from -16 to 16
- norm_gain: float32 [2048], P('tp'), may hold values from 0.1 to 1.9
- in_weight: bfloat16 [2048, 1024], P('fs', 'tp'), may hold values from -0.125 to 0.125
- pool_weight: bfloat16 [8, 128, 128], P('tp'), may hold values from -0.5 to 0.5
- pool_scale: float32 [1024], P('tp'), may hold values from 0.1 to 1.9
- out_weight: bfloat16 [1024, 2048], P('fs', 'tp'), may hold values from -0.1875 to 0.1875
- ffn_gain: float32 [2048], P('tp'), may hold values from 0.1 to 1.9
- gate_weight: bfloat16 [2048, 5632], P('fs', 'tp'), may hold values from -0.125 to 0.125
- up_weight: bfloat16 [2048, 5632], P('fs', 'tp'), may hold values from -0.125 to 0.125
- down_weight: bfloat16 [5632, 2048], P('tp', 'fs'), may hold values from -0.078125 to 0.078125
Outputs:
- output: bfloat16 [8, 384, 2048], P(('grp', 'fs'), None, 'tp'), parts along dimension 0
There are 2 independent parts, one for each index of `grp`. A program takes and returns all parts, laid end to end along the dimension named above; an argument that names none is the same for every part. Nothing has to cross between parts.
All inputs are finite; a program needn't handle non-finite values.
Results may differ from a plain program's by a relative error of at most 0.009.
Values may be sent and summed in bfloat16 or wider, within the bound.
A program may use at most 64 MiB of HBM per device.

v0:
```python
import jax
import jax.numpy as jnp
from jax import lax
from jax.sharding import PartitionSpec as P

D = 2048
GD = 128
EPSILON = 0.05
HALVES = (1, 2, 4, 8)


def local(
    tokens,
    norm_gain,
    in_weight,
    pool_weight,
    pool_scale,
    out_weight,
    ffn_gain,
    gate_weight,
    up_weight,
    down_weight,
):
    seq_local, length, feat_local = tokens.shape
    stream = tokens.astype(jnp.float32)
    first_square = lax.psum(jnp.sum(stream * stream, axis=-1), "tp")
    normed = (stream * lax.rsqrt(first_square[..., None] / D + EPSILON) * norm_gain).astype(
        jnp.bfloat16
    )
    in_full = lax.all_gather(in_weight, "fs", axis=0, tiled=True)
    channels = in_full.shape[1]
    weight_rows = in_full
    pool_input = jnp.einsum(
        "slk,kc->slc",
        lax.all_gather(normed, "tp", axis=2, tiled=True),
        weight_rows,
        preferred_element_type=jnp.float32,
    ).astype(jnp.bfloat16)
    pool_float = pool_input.astype(jnp.float32)
    group_local = pool_weight.shape[0]
    group_ids = lax.axis_index("tp") * group_local + jnp.arange(channels) // GD
    selector = group_ids % 4
    running = jnp.concatenate(
        [jnp.zeros((seq_local, 1, channels), jnp.float32), jnp.cumsum(pool_float, axis=1)], axis=1
    )
    position = jnp.arange(length)
    window_mean = jnp.zeros_like(pool_float)
    for window_index, half_width in enumerate(HALVES):
        upper_sum = jnp.concatenate(
            [running[:, half_width:], jnp.repeat(running[:, -1:], half_width, axis=1)], axis=1
        )[:, :length]
        lower_sum = jnp.concatenate(
            [
                jnp.zeros((seq_local, half_width, channels), jnp.float32),
                running[:, : length + 1 - half_width],
            ],
            axis=1,
        )[:, :length]
        counts = (
            jnp.minimum(position + half_width, length) - jnp.maximum(position - half_width, 0)
        ).astype(jnp.float32)
        window_mean = jnp.where(
            selector == window_index, (upper_sum - lower_sum) / counts[:, None], window_mean
        )
    deviation = (window_mean - pool_float).astype(jnp.bfloat16)
    grouped = deviation.reshape(seq_local, length, group_local, GD)
    mapped = jnp.einsum("slgc,gcd->slgd", grouped, pool_weight, preferred_element_type=jnp.float32)
    pooled = (mapped.reshape(seq_local, length, channels) * pool_scale).astype(jnp.bfloat16)
    out_full = lax.all_gather(out_weight, "fs", axis=0, tiled=True)
    weight_rows = out_full
    mixed = stream + jnp.einsum(
        "jut,tx->jux",
        lax.all_gather(pooled, "tp", axis=2, tiled=True),
        weight_rows,
        preferred_element_type=jnp.float32,
    )
    second_square = lax.psum(jnp.sum(mixed * mixed, axis=-1), "tp")
    normed_two = (mixed * lax.rsqrt(second_square[..., None] / D + EPSILON) * ffn_gain).astype(
        jnp.bfloat16
    )
    features_full = lax.all_gather(normed_two, "tp", axis=2, tiled=True)
    gate_sum = jnp.einsum(
        "slk,kf->slf",
        features_full,
        lax.all_gather(gate_weight, "fs", axis=0, tiled=True),
        preferred_element_type=jnp.float32,
    )
    up_sum = jnp.einsum(
        "slk,kf->slf",
        features_full,
        lax.all_gather(up_weight, "fs", axis=0, tiled=True),
        preferred_element_type=jnp.float32,
    )
    hidden = (jax.nn.silu(gate_sum) * up_sum).astype(jnp.bfloat16)
    partial_value = jnp.einsum(
        "hor,rn->hon",
        hidden,
        lax.all_gather(down_weight, "fs", axis=1, tiled=True),
        preferred_element_type=jnp.float32,
    )
    summed = lax.psum_scatter(
        partial_value.astype(jnp.bfloat16), "tp", scatter_dimension=2, tiled=True
    ).astype(jnp.float32)
    return (mixed + summed).astype(jnp.bfloat16)


def solution(mesh):
    return jax.shard_map(
        local,
        mesh=mesh,
        in_specs=(
            P(("grp", "fs"), None, "tp"),
            P("tp"),
            P("fs", "tp"),
            P("tp", None, None),
            P("tp"),
            P("fs", "tp"),
            P("tp"),
            P("fs", "tp"),
            P("fs", "tp"),
            P("tp", "fs"),
        ),
        out_specs=P(("grp", "fs"), None, "tp"),
        check_vma=False,
    )
```

profile of v0, /device:TPU:0, one launch (start us, length us, event | category | flops | bytes accessed | tf_op | source)
XLA Modules:
  0.0 485.2 jit_solution(12671679941246397171)
XLA Ops:
  6.5 0.0 copy-start
  6.5 0.0 all-gather.10.cloned.1.call-start
  6.5 0.7 all-gather.10.cloned.1.call-update
  7.3 0.0 all-gather.8.cloned.1.call-start
  7.3 1.2 fusion.17
  8.5 8.4 %psum.14 = f32[1,384]{1,0:T(1,128)S(1)} all-reduce(f32[1,384]{1,0:T(1,128)S(1)} %reduce_sum.23), channel_id=1, replica_groups=mesh['grp'=2,'fs'=4,'tp'=4] {'tp'}, use_global_device_ids=true, to_apply=%region_1.0 | all-reduce | flops 384 | bytes 3072 | tf_op jit(solution)/shard_map/psum | solution.py:26
  16.9 1.9 fusion.19
  18.8 0.0 all-gather.8.cloned.1.call-update
  18.8 0.0 all-gather.12.cloned.1.call-start
  18.8 0.7 all-gather.12.cloned.1.call-update
  19.5 0.0 all-gather.14.cloned.1.call-start
  19.6 20.0 %all-gather.10.cloned.1.call-done = bf16[2048,256]{1,0:T(8,128)(2,1)} async-done(((bf16[512,256]{1,0:T(8,128)(2,1)}), bf16[2048,256]{1,0:T(8,128)(2,1)}) %all-gather.10.cloned.1.call-update) | async-done | bytes 1048592 | tf_op jit(solution)/shard_map/all_gather | solution.py:30
  39.6 20.6 %all-gather.8.cloned.1.call-done = bf16[1,384,2048]{2,1,0:T(8,128)(2,1)} async-done(((bf16[1,384,512]{2,1,0:T(8,128)(2,1)}), bf16[1,384,2048]{2,1,0:T(8,128)(2,1)}) %all-gather.8.cloned.1.call-update) | async-done | bytes 1572880 | tf_op jit(solution)/shard_map/all_gather | solution.py:35
  60.2 2.3 fusion.14
  62.5 0.3 fusion.23
  62.8 0.1 copy.12
  63.0 0.1 fusion.63
  63.1 0.1 fusion.61
  63.1 0.1 fusion.62
  63.2 0.0 copy-start.3
  63.3 0.5 fusion.39
  63.8 0.0 copy-start.1
  63.8 0.1 reshape.225
  63.8 0.0 copy-done
  63.8 0.3 fusion.40
  64.1 0.0 copy-done.3
  64.1 0.1 fusion.38
  64.2 0.0 copy-start.2
  64.2 8.6 %all_gather.26 = bf16[1,384,1024]{1,2,0:T(8,128)(2,1)S(1)} all-gather(bf16[1,384,256]{1,2,0:T(8,128)(2,1)S(1)} %fusion.38), channel_id=1, replica_groups=mesh['grp'=2,'fs'=4,'tp'=4] {'tp'}, dimensions={2}, use_global_device_ids=true | all-gather | bytes 983040 | tf_op jit(solution)/shard_map/all_gather | solution.py:73
  72.8 17.0 %all-gather.12.cloned.1.call-done = bf16[1024,512]{1,0:T(8,128)(2,1)} async-done(((bf16[256,512]{1,0:T(8,128)(2,1)}), bf16[1024,512]{1,0:T(8,128)(2,1)}) %all-gather.12.cloned.1.call-update) | async-done | bytes 1048592 | tf_op jit(solution)/shard_map/all_gather | solution.py:69
  89.8 0.0 copy-done.1
  89.8 1.9 multiply_reduce_fusion
  91.8 6.1 %psum.15 = f32[1,384]{1,0:T(1,128)S(1)} all-reduce(f32[1,384]{1,0:T(1,128)S(1)} %reduce_sum.25), channel_id=1, replica_groups=mesh['grp'=2,'fs'=4,'tp'=4] {'tp'}, use_global_device_ids=true, to_apply=%region_5.6 | all-reduce | flops 384 | bytes 3072 | tf_op jit(solution)/shard_map/psum | solution.py:77
  97.9 0.0 copy-done.2
  97.9 0.9 multiply_convert_fusion
  98.8 0.0 all-gather.14.cloned.1.call-update
  98.8 0.0 all-gather.16.cloned.1.call-start
  98.8 0.5 all-gather.16.cloned.1.call-update
  99.4 0.0 all-gather.18.cloned.1.call-start
  99.4 0.5 all-gather.18.cloned.1.call-update
  99.9 0.0 all-gather.20.cloned.1.call-start
  100.0 0.7 all-gather.20.cloned.1.call-update
  100.7 0.0 reduce-scatter.2.cloned.1.call-start
  100.7 17.0 %all-gather.14.cloned.1.call-done = bf16[1,384,2048]{2,1,0:T(8,128)(2,1)} async-done(((bf16[1,384,512]{2,1,0:T(8,128)(2,1)}), bf16[1,384,2048]{2,1,0:T(8,128)(2,1)}) %all-gather.14.cloned.1.call-update) | async-done | bytes 1572880 | tf_op jit(solution)/shard_map/all_gather | solution.py:81
  117.8 0.0 copy-start.4
  117.8 108.1 %all-gather.16.cloned.1.call-done = bf16[2048,1408]{1,0:T(8,128)(2,1)} async-done(((bf16[512,1408]{1,0:T(8,128)(2,1)}), bf16[2048,1408]{1,0:T(8,128)(2,1)}) %all-gather.16.cloned.1.call-update) | async-done | bytes 5767184 | tf_op jit(solution)/shard_map/all_gather | solution.py:85
  225.9 7.1 %fusion.3 = f32[384,1408]{1,0:T(8,128)} fusion(bf16[2048,1408]{1,0:T(8,128)(2,1)} %all-gather.16.cloned.1.call-done, bf16[1,384,2048]{2,1,0:T(8,128)(2,1)} %all-gather.14.cloned.1.call-done), kind=kOutput, calls=%fused_computation.5 | convolution fusion | flops 2214592512 | bytes 9502720 | tf_op jit(solution)/shard_map/slk,kf->slf/dot_general | solution.py:82
  233.0 99.3 %all-gather.18.cloned.1.call-done = bf16[2048,1408]{1,0:T(8,128)(2,1)} async-done(((bf16[512,1408]{1,0:T(8,128)(2,1)}), bf16[2048,1408]{1,0:T(8,128)(2,1)}) %all-gather.18.cloned.1.call-update) | async-done | bytes 5767184 | tf_op jit(solution)/shard_map/all_gather | solution.py:91
  332.3 106.5 %all-gather.20.cloned.1.call-done = bf16[1408,2048]{1,0:T(8,128)(2,1)} async-done(((bf16[1408,512]{1,0:T(8,128)(2,1)}), bf16[1408,2048]{1,0:T(8,128)(2,1)}) %all-gather.20.cloned.1.call-update) | async-done | bytes 5767184 | tf_op jit(solution)/shard_map/all_gather | solution.py:98
  438.9 0.0 copy-done.4
  438.9 11.3 %fusion.1 = bf16[1,384,2048]{2,1,0:T(8,128)(2,1)} fusion(bf16[1408,2048]{1,0:T(8,128)(2,1)} %all-gather.20.cloned.1.call-done, bf16[2048,1408]{1,0:T(8,128)(2,1)} %all-gather.18.cloned.1.call-done, f32[384,1408]{1,0:T(8,128)} %fusion.3, bf16[1,384,2048]{2,1,0:T(8,128)(2,1)S(1)} %copy-done.4), kind=kOutput, calls=%fused_computation.3 | convolution fusion | flops 4433215488 | bytes 16842752 | tf_op jit(solution)/shard_map/hor,rn->hon/dot_general | solution.py:95
  450.1 0.0 reduce-scatter.2.cloned.1.call-update
  450.2 26.4 %reduce-scatter.2.cloned.1.call-done = bf16[1,384,512]{2,1,0:T(8,128)(2,1)} async-done(((bf16[1,384,2048]{2,1,0:T(8,128)(2,1)}), bf16[1,384,512]{2,1,0:T(8,128)(2,1)}) %reduce-scatter.2.cloned.1.call-update) | async-done | bytes 393232 | tf_op jit(solution)/shard_map/reduce_scatter | solution.py:101
  476.5 1.9 add_convert_fusion
  (17 shorter events, 0.2 us)
Async XLA Ops:
  6.5 57.3 %copy-start = (bf16[2,128,128]{2,1,0:T(8,128)(2,1)S(1)}, bf16[2,128,128]{2,1,0:T(8,128)(2,1)}, u32[]{:S(2)}) copy-start(bf16[2,128,128]{2,1,0:T(8,128)(2,1)} %param.13) | copy-start | bytes 196612
  6.5 33.1 %all-gather.10.cloned.1.call-start = ((), (), s32[]{:S(2)}) async-start(), calls=%async_computation.2 | async-start | bytes 1310720 | tf_op jit(solution)/shard_map/all_gather | solution.py:30
  7.3 53.0 %all-gather.8.cloned.1.call-start = ((), (), s32[]{:S(2)}) async-start(), calls=%async_computation.1 | async-start | bytes 1966080 | tf_op jit(solution)/shard_map/all_gather | solution.py:35
  18.8 71.0 %all-gather.12.cloned.1.call-start = ((), (), s32[]{:S(2)}) async-start(), calls=%async_computation.3 | async-start | bytes 1310720 | tf_op jit(solution)/shard_map/all_gather | solution.py:69
  19.5 98.3 %all-gather.14.cloned.1.call-start = ((), (), s32[]{:S(2)}) async-start(), calls=%async_computation.4 | async-start | bytes 1966080 | tf_op jit(solution)/shard_map/all_gather | solution.py:81
  63.2 0.9 copy-start.3
  63.8 26.1 %copy-start.1 = (bf16[1,384,512]{2,1,0:T(8,128)(2,1)S(1)}, bf16[1,384,512]{2,1,0:T(8,128)(2,1)}, u32[]{:S(2)}) copy-start(bf16[1,384,512]{2,1,0:T(8,128)(2,1)} %param.10) | copy-start | bytes 1179652
  64.2 33.6 %copy-start.2 = (f32[512]{0:T(512)S(1)}, f32[512]{0:T(512)}, u32[]{:S(2)}) copy-start(f32[512]{0:T(512)} %param.16) | copy-start | bytes 6148
  98.8 127.2 %all-gather.16.cloned.1.call-start = ((), (), s32[]{:S(2)}) async-start(), calls=%async_computation.5 | async-start | bytes 7208960 | tf_op jit(solution)/shard_map/all_gather | solution.py:85
  99.4 233.0 %all-gather.18.cloned.1.call-start = ((), (), s32[]{:S(2)}) async-start(), calls=%async_computation.6 | async-start | bytes 7208960 | tf_op jit(solution)/shard_map/all_gather | solution.py:91
  99.9 338.9 %all-gather.20.cloned.1.call-start = ((), (), s32[]{:S(2)}) async-start(), calls=%async_computation.7 | async-start | bytes 7208960 | tf_op jit(solution)/shard_map/all_gather | solution.py:98
  100.7 375.8 %reduce-scatter.2.cloned.1.call-start = ((), (), s32[]{:S(2)}) async-start(), calls=%async_computation.8 | async-start | bytes 1966080 | tf_op jit(solution)/shard_map/reduce_scatter | solution.py:101
  117.8 321.1 %copy-start.4 = (bf16[1,384,2048]{2,1,0:T(8,128)(2,1)S(1)}, bf16[1,384,2048]{2,1,0:T(8,128)(2,1)}, u32[]{:S(2)}) copy-start(bf16[1,384,2048]{2,1,0:T(8,128)(2,1)} %all-gather.14.cloned.1.call-done) | copy-start | bytes 4718596
Sparse Core Ops, SparseCore 0:
  8.9 30.6 all-gather.9
  41.2 18.9 all-gather.7
  61.8 27.9 all-gather.11
  98.9 18.8 all-gather.13
  119.2 106.6 all-gather.15
  227.4 104.9 all-gather.17
  333.9 104.9 all-gather.19
  450.3 26.2 reduce-scatter.1
where the time goes:
time: 486 us; the launch traced here: 485 us
  waiting for transfers between devices  418 us (86%)
  blocking collectives  23 us (5%)
  matrix products  22.8 us (5%)
  between operations  13.7 us (3%)
  other arithmetic  6.86 us (1%)
    all_gather x1, waiting for transfers between devices, local(): lax.all_gather(gate_weight, 'fs', axis=0, tiled=True)  108 us
    all_gather x1, waiting for transfers between devices, local(): lax.all_gather(down_weight, 'fs', axis=1, tiled=True)  107 us
    all_gather x1, waiting for transfers between devices, local(): lax.all_gather(up_weight, 'fs', axis=0, tiled=True)  99.3 us
    reduce_scatter x1, waiting for transfers between devices, local(): lax.psum_scatter(partial_value.astype(jnp.bfloat16), 'tp', scatter_dimens...  26.4 us
    all_gather x1, waiting for transfers between devices, local(): lax.all_gather(normed, 'tp', axis=2, tiled=True)  20.6 us
    all_gather x1, waiting for transfers between devices, local(): in_full = lax.all_gather(in_weight, 'fs', axis=0, tiled=True)  20 us
    all_gather x1, waiting for transfers between devices, local(): features_full = lax.all_gather(normed_two, 'tp', axis=2, tiled=True)  17 us
    all_gather x1, waiting for transfers between devices, local(): out_full = lax.all_gather(out_weight, 'fs', axis=0, tiled=True)  17 us
  transfers between devices with their start and end apart: 8, of which 8 were waited for; matrix products, arithmetic and copies ran while one was open for 3% of the time, Pallas kernels for 0%

commit v1 on v0

--- a/solution.py
+++ b/solution.py
@@ -7,6 +7,22 @@
 GD = 128
 EPSILON = 0.05
 HALVES = (1, 2, 4, 8)
+
+
+def summed_both_ways(shard, axis, dim, term):
+    peers, index, rows = (lax.axis_size(axis), lax.axis_index(axis), shard.shape[dim])
+    upward = [(i, (i + 1) % peers) for i in range(peers)]
+    behind = [(i, (i - 1) % peers) for i in range(peers)]
+    halfway = peers // 2
+    from_left = from_right = shard
+    total = term(shard, index * rows)
+    for step in range(1, halfway + 1):
+        from_left = lax.ppermute(from_left, axis, upward)
+        if step < peers - halfway:
+            from_right = lax.ppermute(from_right, axis, behind)
+            total = total + term(from_right, (index + step) % peers * rows)
+        total = total + term(from_left, (index - step) % peers * rows)
+    return total
 
 
 def local(
@@ -85,11 +101,16 @@
         lax.all_gather(gate_weight, "fs", axis=0, tiled=True),
         preferred_element_type=jnp.float32,
     )
-    up_sum = jnp.einsum(
-        "slk,kf->slf",
-        features_full,
-        lax.all_gather(up_weight, "fs", axis=0, tiled=True),
-        preferred_element_type=jnp.float32,
+    up_sum = summed_both_ways(
+        up_weight,
+        "fs",
+        0,
+        lambda shard, offset: jnp.einsum(
+            "slk,kf->slf",
+            lax.dynamic_slice_in_dim(features_full, offset, shard.shape[0], axis=2),
+            shard,
+            preferred_element_type=jnp.float32,
+        ),
     )
     hidden = (jax.nn.silu(gate_sum) * up_sum).astype(jnp.bfloat16)
     partial_value = jnp.einsum(

time: 486 us -> 440 us (0.905)
  waiting for transfers between devices: 418 us -> 352 us
  starting transfers between devices: 0.28 us -> 17.4 us
    ppermute x0 -> x3, waiting for transfers between devices: none -> 134 us  [the longest x1 97.8 us: summed_both_ways(): from_right = lax.ppermute(from_right, axis, behind)]
    all_gather x1 -> x0, waiting for transfers between devices: 99.3 us -> none  [local(): lax.all_gather(up_weight, 'fs', axis=0, tiled=True)]
    all_gather x1, waiting for transfers between devices: 108 us -> 31.8 us  [local(): lax.all_gather(gate_weight, 'fs', axis=0, tiled=True)]
    ppermute x0 -> x3, starting transfers between devices: none -> 17.1 us  [the longest x2 14.5 us: summed_both_ways(): from_left = lax.ppermute(from_left, axis, upward)]
    all_gather x1, waiting for transfers between devices: 17 us -> 0.01 us  [local(): features_full = lax.all_gather(normed_two, 'tp', axis=2, tiled=True)]
    all_gather x1, waiting for transfers between devices: 107 us -> 99.7 us  [local(): lax.all_gather(down_weight, 'fs', axis=1, tiled=True)]
    dot_general x0 -> x3, matrix products: none -> 6.22 us  [local(): jnp.einsum('slk,kf->slf', lax.dynamic_slice_in_dim(features_full, offset,...]
  transfers between devices with their start and end apart: 8 -> 10, of which waited for: 8 -> 8; matrix products, arithmetic and copies ran while one was open for 3% -> 5% of each run, Pallas kernels for 0% -> 0%
where the time goes in v1:
time: 440 us
  waiting for transfers between devices  352 us (80%)
  matrix products  26.2 us (6%)
  blocking collectives  23 us (5%)
  starting transfers between devices  17.4 us (4%)
  between operations  13.7 us (3%)
  other arithmetic  6.85 us (2%)
    all_gather x1, waiting for transfers between devices, local(): lax.all_gather(down_weight, 'fs', axis=1, tiled=True)  99.7 us
    ppermute x1, waiting for transfers between devices, summed_both_ways(): from_right = lax.ppermute(from_right, axis, behind)  97.8 us
    ppermute x2, waiting for transfers between devices, summed_both_ways(): from_left = lax.ppermute(from_left, axis, upward)  36.4 us
    all_gather x1, waiting for transfers between devices, local(): lax.all_gather(gate_weight, 'fs', axis=0, tiled=True)  31.8 us
    reduce_scatter x1, waiting for transfers between devices, local(): lax.psum_scatter(partial_value.astype(jnp.bfloat16), 'tp', scatter_dimens...  26.4 us
    all_gather x1, waiting for transfers between devices, local(): lax.all_gather(normed, 'tp', axis=2, tiled=True)  20.6 us
    all_gather x1, waiting for transfers between devices, local(): in_full = lax.all_gather(in_weight, 'fs', axis=0, tiled=True)  20 us
    all_gather x1, waiting for transfers between devices, local(): out_full = lax.all_gather(out_weight, 'fs', axis=0, tiled=True)  17 us
  transfers between devices with their start and end apart: 10, of which 8 were waited for; matrix products, arithmetic and copies ran while one was open for 5% of the time, Pallas kernels for 0%

profile of v1, /device:TPU:0, one launch (start us, length us, event | category | flops | bytes accessed | tf_op | source)
XLA Modules:
  0.0 439.8 jit_solution(17073644510114031916)
XLA Ops:
  6.5 0.0 copy-start
  6.5 0.0 all-gather.9.cloned.1.call-start
  6.5 0.7 all-gather.9.cloned.1.call-update
  7.3 0.0 all-gather.7.cloned.1.call-start
  7.3 1.2 fusion.18
  8.5 8.4 %psum.14 = f32[1,384]{1,0:T(1,128)S(1)} all-reduce(f32[1,384]{1,0:T(1,128)S(1)} %reduce_sum.23), channel_id=1, replica_groups=mesh['grp'=2,'fs'=4,'tp'=4] {'tp'}, use_global_device_ids=true, to_apply=%region_1.0 | all-reduce | flops 384 | bytes 3072 | tf_op jit(solution)/shard_map/psum | solution.py:42
  16.9 1.9 fusion.20
  18.8 0.0 all-gather.7.cloned.1.call-update
  18.8 0.0 all-gather.11.cloned.1.call-start
  18.8 0.7 all-gather.11.cloned.1.call-update
  19.5 0.0 all-gather.13.cloned.1.call-start
  19.6 20.0 %all-gather.9.cloned.1.call-done = bf16[2048,256]{1,0:T(8,128)(2,1)} async-done(((bf16[512,256]{1,0:T(8,128)(2,1)}), bf16[2048,256]{1,0:T(8,128)(2,1)}) %all-gather.9.cloned.1.call-update) | async-done | bytes 1048592 | tf_op jit(solution)/shard_map/all_gather | solution.py:46
  39.6 20.6 %all-gather.7.cloned.1.call-done = bf16[1,384,2048]{2,1,0:T(8,128)(2,1)} async-done(((bf16[1,384,512]{2,1,0:T(8,128)(2,1)}), bf16[1,384,2048]{2,1,0:T(8,128)(2,1)}) %all-gather.7.cloned.1.call-update) | async-done | bytes 1572880 | tf_op jit(solution)/shard_map/all_gather | solution.py:51
  60.2 2.3 fusion.14
  62.5 0.3 fusion.22
  62.8 0.1 copy.12
  63.0 0.1 fusion.78
  63.1 0.1 fusion.76
  63.1 0.1 fusion.77
  63.2 0.0 copy-start.5
  63.3 0.5 fusion.49
  63.8 0.0 copy-start.1
  63.8 0.1 reshape.242
  63.8 0.0 copy-done
  63.8 0.3 fusion.50
  64.1 0.0 copy-done.5
  64.1 0.1 fusion.37
  64.2 8.6 %all_gather.23 = bf16[1,384,1024]{1,2,0:T(8,128)(2,1)S(1)} all-gather(bf16[1,384,256]{1,2,0:T(8,128)(2,1)S(1)} %fusion.37), channel_id=1, replica_groups=mesh['grp'=2,'fs'=4,'tp'=4] {'tp'}, dimensions={2}, use_global_device_ids=true | all-gather | bytes 983040 | tf_op jit(solution)/shard_map/all_gather | solution.py:89
  72.8 0.0 copy-start.4
  72.8 17.0 %all-gather.11.cloned.1.call-done = bf16[1024,512]{1,0:T(8,128)(2,1)} async-done(((bf16[256,512]{1,0:T(8,128)(2,1)}), bf16[1024,512]{1,0:T(8,128)(2,1)}) %all-gather.11.cloned.1.call-update) | async-done | bytes 1048592 | tf_op jit(solution)/shard_map/all_gather | solution.py:85
  89.8 0.0 copy-done.1
  89.8 1.9 multiply_reduce_fusion
  91.8 6.1 %psum.15 = f32[1,384]{1,0:T(1,128)S(1)} all-reduce(f32[1,384]{1,0:T(1,128)S(1)} %reduce_sum.25), channel_id=1, replica_groups=mesh['grp'=2,'fs'=4,'tp'=4] {'tp'}, use_global_device_ids=true, to_apply=%region_5.6 | all-reduce | flops 384 | bytes 3072 | tf_op jit(solution)/shard_map/psum | solution.py:93
  97.9 0.0 copy-done.4
  97.9 0.9 multiply_convert_fusion
  98.8 0.0 copy-start.2
  98.8 0.0 all-gather.13.cloned.1.call-update
  98.8 0.0 all-gather.15.cloned.1.call-start
  98.8 0.5 all-gather.15.cloned.1.call-update
  99.4 0.0 all-gather.17.cloned.1.call-start
  99.4 0.5 all-gather.17.cloned.1.call-update
  100.0 0.0 reduce-scatter.2.cloned.1.call-start
  100.0 0.1 copy-done.2
  100.1 1.1 collective-permute-start.1
  101.3 2.7 collective-permute-start
  103.9 36.4 %collective-permute-done.1 = bf16[512,1408]{1,0:T(8,128)(2,1)} collective-permute-done((bf16[512,1408]{1,0:T(8,128)(2,1)S(1)}, bf16[512,1408]{1,0:T(8,128)(2,1)}, u32[]{:S(2)}, u32[]{:S(2)}) %collective-permute-start.1) | collective-permute-done | bytes 1441824 | tf_op jit(solution)/shard_map/ppermute | solution.py:20
  140.3 13.3 %collective-permute-start.2 = (bf16[512,1408]{1,0:T(8,128)(2,1)}, bf16[512,1408]{1,0:T(8,128)(2,1)}, u32[]{:S(2)}, u32[]{:S(2)}) collective-permute-start(bf16[512,1408]{1,0:T(8,128)(2,1)} %collective-permute-done.1), channel_id=1, source_target_pairs={{0,4},{4,8},{8,12},{12,0},{1,5},{5,9},{9,13},{13,1},{2,6},{6,10},{... | collective-permute-start | bytes 4325384 | tf_op jit(solution)/shard_map/ppermute | solution.py:20
  153.7 0.0 all-gather.13.cloned.1.call-done
  153.7 0.0 copy-start.3
  153.7 1.9 fusion.42
  155.5 97.8 %collective-permute-done = bf16[512,1408]{1,0:T(8,128)(2,1)} collective-permute-done((bf16[512,1408]{1,0:T(8,128)(2,1)S(1)}, bf16[512,1408]{1,0:T(8,128)(2,1)}, u32[]{:S(2)}, u32[]{:S(2)}) %collective-permute-start) | collective-permute-done | bytes 1441824 | tf_op jit(solution)/shard_map/ppermute | solution.py:22
  253.4 0.0 copy-done.3
  253.4 2.2 convolution_add_fusion.2
  255.5 2.2 convolution_add_fusion.1
  257.7 31.8 %all-gather.15.cloned.1.call-done = bf16[2048,1408]{1,0:T(8,128)(2,1)} async-done(((bf16[512,1408]{1,0:T(8,128)(2,1)}), bf16[2048,1408]{1,0:T(8,128)(2,1)}) %all-gather.15.cloned.1.call-update) | async-done | bytes 5767184 | tf_op jit(solution)/shard_map/all_gather | solution.py:101
  289.5 7.2 %fusion.3 = f32[384,1408]{1,0:T(8,128)} fusion(bf16[2048,1408]{1,0:T(8,128)(2,1)} %all-gather.15.cloned.1.call-done, bf16[1,384,2048]{2,1,0:T(8,128)(2,1)} %all-gather.13.cloned.1.call-done), kind=kOutput, calls=%fused_computation.7 | convolution fusion | flops 2214592512 | bytes 9502720 | tf_op jit(solution)/shard_map/slk,kf->slf/dot_general | solution.py:98
  296.7 0.0 collective-permute-done.2
  296.7 99.7 %all-gather.17.cloned.1.call-done = bf16[1408,2048]{1,0:T(8,128)(2,1)} async-done(((bf16[1408,512]{1,0:T(8,128)(2,1)}), bf16[1408,2048]{1,0:T(8,128)(2,1)}) %all-gather.17.cloned.1.call-update) | async-done | bytes 5767184 | tf_op jit(solution)/shard_map/all_gather | solution.py:119
  396.4 8.3 %fusion.2 = bf16[1,384,2048]{2,1,0:T(8,128)(2,1)} fusion(bf16[1408,2048]{1,0:T(8,128)(2,1)} %all-gather.17.cloned.1.call-done, f32[384,1408]{1,0:T(8,128)S(1)} %convolution_add_fusion.1, bf16[512,1408]{1,0:T(8,128)(2,1)} %collective-permute-done.2, f32[384,1408]{1,0:T(8,128)} %fusion.3, bf16[1,384,2048]{2,1,0:T(8,128)(2,1)} %all-gather.13.cloned.1.call-done, ...), kind=kOutput, calls=%fused_computation.6 | convolution fusion | flops 2772811776 | bytes 13500420 | tf_op jit(solution)/shard_map/hor,rn->hon/dot_general | solution.py:116
  404.7 0.0 reduce-scatter.2.cloned.1.call-update
  404.7 26.4 %reduce-scatter.2.cloned.1.call-done = bf16[1,384,512]{2,1,0:T(8,128)(2,1)} async-done(((bf16[1,384,2048]{2,1,0:T(8,128)(2,1)}), bf16[1,384,512]{2,1,0:T(8,128)(2,1)}) %reduce-scatter.2.cloned.1.call-update) | async-done | bytes 393232 | tf_op jit(solution)/shard_map/reduce_scatter | solution.py:122
  431.1 1.9 add_convert_fusion
  (17 shorter events, 0.2 us)
Async XLA Ops:
  6.5 57.3 %copy-start = (bf16[2,128,128]{2,1,0:T(8,128)(2,1)S(1)}, bf16[2,128,128]{2,1,0:T(8,128)(2,1)}, u32[]{:S(2)}) copy-start(bf16[2,128,128]{2,1,0:T(8,128)(2,1)} %param.13) | copy-start | bytes 196612
  6.5 33.1 %all-gather.9.cloned.1.call-start = ((), (), s32[]{:S(2)}) async-start(), calls=%async_computation.2 | async-start | bytes 1310720 | tf_op jit(solution)/shard_map/all_gather | solution.py:46
  7.3 53.0 %all-gather.7.cloned.1.call-start = ((), (), s32[]{:S(2)}) async-start(), calls=%async_computation.1 | async-start | bytes 1966080 | tf_op jit(solution)/shard_map/all_gather | solution.py:51
  18.8 71.0 %all-gather.11.cloned.1.call-start = ((), (), s32[]{:S(2)}) async-start(), calls=%async_computation.3 | async-start | bytes 1310720 | tf_op jit(solution)/shard_map/all_gather | solution.py:85
  19.5 134.1 %all-gather.13.cloned.1.call-start = ((), (), s32[]{:S(2)}) async-start(), calls=%async_computation.4 | async-start | bytes 1966080 | tf_op jit(solution)/shard_map/all_gather | solution.py:97
  63.2 0.9 copy-start.5
  63.8 26.1 %copy-start.1 = (bf16[1,384,512]{2,1,0:T(8,128)(2,1)S(1)}, bf16[1,384,512]{2,1,0:T(8,128)(2,1)}, u32[]{:S(2)}) copy-start(bf16[1,384,512]{2,1,0:T(8,128)(2,1)} %param.10) | copy-start | bytes 1179652
  72.8 25.1 %copy-start.4 = (f32[512]{0:T(512)S(1)}, f32[512]{0:T(512)}, u32[]{:S(2)}) copy-start(f32[512]{0:T(512)} %param.16) | copy-start | bytes 6148
  98.8 1.4 copy-start.2
  98.8 190.7 %all-gather.15.cloned.1.call-start = ((), (), s32[]{:S(2)}) async-start(), calls=%async_computation.5 | async-start | bytes 7208960 | tf_op jit(solution)/shard_map/all_gather | solution.py:101
  99.4 297.0 %all-gather.17.cloned.1.call-start = ((), (), s32[]{:S(2)}) async-start(), calls=%async_computation.6 | async-start | bytes 7208960 | tf_op jit(solution)/shard_map/all_gather | solution.py:119
  100.0 331.2 %reduce-scatter.2.cloned.1.call-start = ((), (), s32[]{:S(2)}) async-start(), calls=%async_computation.7 | async-start | bytes 1966080 | tf_op jit(solution)/shard_map/reduce_scatter | solution.py:122
  100.1 40.2 %collective-permute-start.1 = (bf16[512,1408]{1,0:T(8,128)(2,1)S(1)}, bf16[512,1408]{1,0:T(8,128)(2,1)}, u32[]{:S(2)}, u32[]{:S(2)}) collective-permute-start(bf16[512,1408]{1,0:T(8,128)(2,1)S(1)} %copy-done.2), channel_id=1, source_target_pairs={{0,4},{4,8},{8,12},{12,0},{1,5},{5,9},{9,13},{13,1},{2,6},{6,10},{... | collective-permute-start | bytes 4325384 | tf_op jit(solution)/shard_map/ppermute | solution.py:20
  101.3 152.1 %collective-permute-start = (bf16[512,1408]{1,0:T(8,128)(2,1)S(1)}, bf16[512,1408]{1,0:T(8,128)(2,1)}, u32[]{:S(2)}, u32[]{:S(2)}) collective-permute-start(bf16[512,1408]{1,0:T(8,128)(2,1)S(1)} %copy-done.2), channel_id=1, source_target_pairs={{0,12},{4,0},{8,4},{12,8},{1,13},{5,1},{9,5},{13,9},{2,14},{6,2},{... | collective-permute-start | bytes 4325384 | tf_op jit(solution)/shard_map/ppermute | solution.py:22
  140.3 156.4 %collective-permute-start.2 = (bf16[512,1408]{1,0:T(8,128)(2,1)}, bf16[512,1408]{1,0:T(8,128)(2,1)}, u32[]{:S(2)}, u32[]{:S(2)}) collective-permute-start(bf16[512,1408]{1,0:T(8,128)(2,1)} %collective-permute-done.1), channel_id=1, source_target_pairs={{0,4},{4,8},{8,12},{12,0},{1,5},{5,9},{9,13},{13,1},{2,6},{6,10},{... | collective-permute-start | bytes 4325384 | tf_op jit(solution)/shard_map/ppermute | solution.py:20
  153.7 99.7 %copy-start.3 = (bf16[1,384,2048]{2,1,0:T(8,128)(2,1)S(1)}, bf16[1,384,2048]{2,1,0:T(8,128)(2,1)}, u32[]{:S(2)}) copy-start(bf16[1,384,2048]{2,1,0:T(8,128)(2,1)} %all-gather.13.cloned.1.call-done) | copy-start | bytes 4718596
Sparse Core Ops, SparseCore 0:
  8.9 30.6 all-gather.8
  41.2 18.9 all-gather.6
  61.8 27.9 all-gather.10
  98.9 18.8 all-gather.12
  119.2 170.2 all-gather.14
  290.9 105.3 all-gather.16
  404.8 26.2 reduce-scatter.1
